TPU v7x, 32 devices: a whole 2x2x4 slice. The times are simulated.
32 devices in a mesh: sp: 16 (over z, y, x), tp: 2 (over core).
Axes of the slice: x: 2, y: 2, z: 4, core: 2. Of those that a mesh axis runs over, the one named last changes fastest.
Arguments:
- tokens: bfloat16 [2048, 2048], P(('sp', 'tp')), may hold values from -6 to 6
- input_norm_gain: float32 [2048], replicated, may hold values from 0.1 to 1.9
- differential_query: bfloat16 [2048, 1024], P(None, 'tp'), may hold values from -0.176776695 to 0.176776695, as said below
- differential_key: bfloat16 [2048, 1024], P(None, 'tp'), may hold values from -0.176776695 to 0.176776695, as said below
- differential_value: bfloat16 [2048, 1024], P(None, 'tp'), may hold values from -0.125 to 0.125
- query_norm_gain: float32 [64], replicated, may hold values from 1.15 to 5
- key_norm_gain: float32 [64], replicated, may hold values from 1.15 to 5
- second_map_weight: float32 [8], P('tp'), may hold values from 0.3 to 0.8
- differential_norm_gain: float32 [128], replicated, may hold values from 0.1 to 1.9
- linear_query: bfloat16 [2048, 512], P(None, 'tp'), may hold values from -0.125 to 0.125
- linear_key: bfloat16 [2048, 512], P(None, 'tp'), may hold values from -0.125 to 0.125
- linear_value: bfloat16 [2048, 1024], P(None, 'tp'), may hold values from -0.125 to 0.125
- linear_output_gate: bfloat16 [2048, 1024], P(None, 'tp'), may hold values from -0.125 to 0.125
- forget_down_factor: bfloat16 [2048, 32], replicated, may hold values from -0.125 to 0.125
- forget_up_factor: bfloat16 [32, 512], P(None, 'tp'), may hold values from -2.109375 to 2.109375
- forget_bias: float32 [512], P('tp'), may hold values from -0.5 to 10
- extra_shrinkage_exponent: float32 [2048, 8], P('sp', 'tp'), may hold values from -1.5 to 0
- linear_norm_gain: float32 [128], replicated, may hold values from 0.1 to 1.9
- differential_output_rows: bfloat16 [1024, 2048], P('tp'), may hold values from -0.125 to 0.125
- linear_output_rows: bfloat16 [1024, 2048], P('tp'), may hold values from -0.125 to 0.125
Outputs:
- layer_out: bfloat16 [2048, 2048], P(('sp', 'tp'))
Inputs may be any that keep to these rules, and one draw needn't show every extreme that they name: `differential_query`: independent entries of scale one over sqrt(2048). `differential_key`: entries of scale one over sqrt(2048).
All inputs are finite; a program needn't handle non-finite values.
Results may differ from a plain program's by a relative error of at most 0.015.
Values may be sent and summed in bfloat16 or wider, within the bound.
A program may use at most 64 MiB of HBM per device.

v0:
```python
from functools import partial
import jax
import jax.numpy as jnp
from jax import lax
from jax.sharding import PartitionSpec as P

HEAD = 64
VDIM = 128
RECURRENT_DIM = 64
GLA_DV = 128
BLOCK = 64
RMS_EPS = 1e-06
SOFTMAX_DIVISOR = 16.0
OUT_SCALE = 0.8
NEG_LARGE = -1e30
HIGHEST = lax.Precision.HIGHEST


def partner(block, axis, apart):
    count = lax.axis_size(axis)
    route = []
    for low in range(count):
        high = low | 1 << apart
        if high != low and high < count:
            route += [(low, high), (high, low)]
    return lax.ppermute(block, axis, route)


def prefix(shard, axis, combine, identity):
    devices, position = (lax.axis_size(axis), lax.axis_index(axis))
    everything = jax.tree.map(lambda part: lax.all_gather(part, axis), shard)
    start = jax.tree.map(
        lambda part, zero: jnp.broadcast_to(jnp.asarray(zero, part.dtype), part.shape),
        shard,
        identity,
    )

    def turn(k, before):
        reached = k < position
        new = combine(before, jax.tree.map(lambda part: part[k], everything))
        return jax.tree.map(lambda a, b: jnp.where(reached, a, b), new, before)

    return lax.fori_loop(0, devices, turn, start)


def rms_scale(values, scale_gain):
    mean_sq = jnp.mean(values * values, axis=-1, keepdims=True)
    return values * lax.rsqrt(mean_sq + RMS_EPS) * scale_gain


def block_length(total_rows, shard_rows):
    best = shard_rows
    shard_total = total_rows // shard_rows
    for multiple in range(1, shard_total + 1):
        if shard_total % multiple == 0 and shard_rows * multiple <= 2048:
            best = shard_rows * multiple
    return best


def combine_chain(earlier, later):
    return (earlier[0] * later[0], earlier[1] * later[0][..., None] + later[1])


def keep_carry(carry_now):
    return carry_now


def attend_span(query_set, query_pos, keys_here, values_here, key_pos, carry_now):
    row_peaks, totals, numerators = carry_now
    query_rows = query_set.shape[0]
    group_count = query_set.shape[1]
    attn_heads = group_count // 2
    span_rows = keys_here.shape[0]
    scores = jnp.einsum(
        "tgd,kgd->gtk", query_set, keys_here, preferred_element_type=jnp.float32
    ) * HEAD ** (-0.5)
    causal = key_pos[None, :] <= query_pos[:, None]
    scores = jnp.where(causal[None], scores, NEG_LARGE)
    new_peaks = jnp.maximum(row_peaks, jnp.max(scores, axis=-1))
    weights = jnp.where(causal[None], jnp.exp(scores - new_peaks[..., None]), 0.0)
    factor = jnp.exp(row_peaks - new_peaks)
    totals = totals * factor + jnp.sum(weights, axis=-1)
    rounded = weights.astype(jnp.bfloat16).reshape(attn_heads, 2, query_rows, span_rows)
    contrib = jnp.einsum(
        "hmtk,khv->hmtv", rounded, values_here, preferred_element_type=jnp.float32
    ).reshape(group_count, query_rows, VDIM)
    return (new_peaks, totals, numerators * factor[..., None] + contrib)


def per_device(
    tokens,
    input_norm_gain,
    differential_query,
    differential_key,
    differential_value,
    query_norm_gain,
    key_norm_gain,
    second_map_weight,
    differential_norm_gain,
    linear_query,
    linear_key,
    linear_value,
    linear_output_gate,
    forget_down_factor,
    forget_up_factor,
    forget_bias,
    extra_shrinkage_exponent,
    linear_norm_gain,
    differential_output_rows,
    linear_output_rows,
):
    sp_size = lax.axis_size("sp")
    sp_index = lax.axis_index("sp")
    attn_heads = second_map_weight.shape[0]
    linear_head_list = extra_shrinkage_exponent.shape[1]
    normed = rms_scale(tokens.astype(jnp.float32), input_norm_gain).astype(jnp.bfloat16)
    parts_list = [
        differential_query,
        differential_key,
        differential_value,
        linear_query,
        linear_key,
        linear_value,
        linear_output_gate,
        forget_down_factor,
    ]
    packed = jnp.concatenate(parts_list, axis=1)
    bounds = [0]
    for matrix in parts_list:
        bounds.append(bounds[-1] + matrix.shape[1])
    projected = jnp.dot(
        lax.all_gather(normed, "tp", axis=0, tiled=True), packed, preferred_element_type=jnp.float32
    ).astype(jnp.bfloat16)
    row_count = projected.shape[0]
    half_rows = row_count // 2
    bit_count = sp_size.bit_length() - 1

    def section(column_set):
        return projected[:, bounds[column_set] : bounds[column_set + 1]]

    group_count = 2 * attn_heads
    query_norm = rms_scale(
        section(0).astype(jnp.float32).reshape(row_count, group_count, HEAD), query_norm_gain
    ).astype(jnp.bfloat16)
    key_norm = rms_scale(
        section(1).astype(jnp.float32).reshape(row_count, group_count, HEAD), key_norm_gain
    ).astype(jnp.bfloat16)
    key_flat = key_norm.reshape(row_count, group_count * HEAD)
    value_flat = section(2)
    far_queries = query_norm[half_rows:].reshape(half_rows, group_count * HEAD)
    for bit in range(bit_count):
        far_queries = partner(far_queries, "sp", bit)
    mirror_index = sp_size - 1 - sp_index
    own_pos = sp_index * row_count + jnp.arange(half_rows, dtype=jnp.int32)
    far_pos = mirror_index * row_count + half_rows + jnp.arange(half_rows, dtype=jnp.int32)
    query_sets = [
        (query_norm[:half_rows], own_pos),
        (far_queries.reshape(half_rows, group_count, HEAD), far_pos),
    ]
    fold_start = tuple(
        (
            (
                jnp.full((group_count, query_set.shape[0]), NEG_LARGE, jnp.float32),
                jnp.zeros((group_count, query_set.shape[0]), jnp.float32),
                jnp.zeros((group_count, query_set.shape[0], VDIM), jnp.float32),
            )
            for query_set, query_pos in query_sets
        )
    )
    key_rows = lax.all_gather(key_flat, "sp", axis=0, tiled=True)
    value_rows = lax.all_gather(value_flat, "sp", axis=0, tiled=True)
    piece_rows = key_rows.shape[0]
    span_rows = block_length(piece_rows, row_count)

    def attend(span_index, carries):
        row_start = span_index * span_rows
        keys_here = lax.dynamic_slice_in_dim(
            key_rows, span_index * span_rows, span_rows, 0
        ).reshape(span_rows, group_count, HEAD)
        values_here = lax.dynamic_slice_in_dim(
            value_rows, span_index * span_rows, span_rows, 0
        ).reshape(span_rows, attn_heads, VDIM)
        key_pos = row_start + jnp.arange(span_rows, dtype=jnp.int32)
        results = []
        for (query_set, query_pos), carry_in in zip(query_sets, carries):
            work = partial(attend_span, query_set, query_pos, keys_here, values_here, key_pos)
            results.append(lax.cond(row_start <= jnp.max(query_pos), work, keep_carry, carry_in))
        return tuple(results)

    folded = lax.fori_loop(0, piece_rows // span_rows, attend, fold_start)

    def finish(carry_set):
        row_peaks, totals, numerators = carry_set
        set_rows = totals.shape[1]
        maps_out = (numerators / totals[..., None]).reshape(attn_heads, 2, set_rows, VDIM)
        attn_mix = maps_out[:, 0] - second_map_weight[:, None, None] * maps_out[:, 1]
        return (
            (rms_scale(attn_mix, differential_norm_gain) * OUT_SCALE)
            .transpose(1, 0, 2)
            .reshape(set_rows, attn_heads * VDIM)
            .astype(jnp.bfloat16)
        )

    own_rows = finish(folded[0])
    far_rows = finish(folded[1])
    for bit in range(bit_count):
        far_rows = partner(far_rows, "sp", bit)
    attn_out = jnp.concatenate([own_rows, far_rows], axis=0)
    chain_queries = section(3).astype(jnp.float32).reshape(
        row_count, linear_head_list, RECURRENT_DIM
    ) * RECURRENT_DIM ** (-0.5)
    chain_keys = section(4).astype(jnp.float32).reshape(row_count, linear_head_list, RECURRENT_DIM)
    chain_values = section(5).astype(jnp.float32).reshape(row_count, linear_head_list, GLA_DV)
    gated = jax.nn.silu(section(6).astype(jnp.float32)).reshape(row_count, linear_head_list, GLA_DV)
    sigmoid_preactivation = (
        jnp.dot(section(7), forget_up_factor, preferred_element_type=jnp.float32) + forget_bias
    )
    shrinkage_exponent = (
        jax.nn.log_sigmoid(sigmoid_preactivation).reshape(
            row_count, linear_head_list, RECURRENT_DIM
        )
        / SOFTMAX_DIVISOR
        + extra_shrinkage_exponent[:, :, None]
    )
    block_total = row_count // BLOCK

    def blockify(array):
        return array.reshape(block_total, BLOCK, linear_head_list, array.shape[-1])

    causal_block = jnp.arange(BLOCK)[:, None] >= jnp.arange(BLOCK)[None, :]

    def chain_block(carry, inputs):
        carried, log_total = carry
        query_block, key_block, value_block, decay_block = inputs
        log_cum = jnp.cumsum(decay_block, axis=0)
        log_last = log_cum[-1]
        query_decayed = query_block * jnp.exp(log_cum)
        key_inverse = key_block * jnp.exp(-log_cum)
        inner_scores = jnp.einsum("thd,shd->hts", query_decayed, key_inverse, precision=HIGHEST)
        inner_scores = jnp.where(causal_block[None], inner_scores, 0.0)
        local_out = jnp.einsum("hts,she->the", inner_scores, value_block, precision=HIGHEST)
        local_out = local_out + jnp.einsum(
            "thd,hde->the", query_decayed, carried, precision=HIGHEST
        )
        key_end = key_block * jnp.exp(log_last[None] - log_cum)
        carried = carried * jnp.exp(log_last)[..., None] + jnp.einsum(
            "thd,the->hde", key_end, value_block, precision=HIGHEST
        )
        carried_query = query_decayed * jnp.exp(log_total)[None]
        return ((carried, log_total + log_last), (local_out, carried_query))

    chain_zero = (
        jnp.zeros((linear_head_list, RECURRENT_DIM, GLA_DV), jnp.float32),
        jnp.zeros((linear_head_list, RECURRENT_DIM), jnp.float32),
    )
    (own_state, log_total), (local_out, carried_query) = lax.scan(
        chain_block,
        chain_zero,
        (
            blockify(chain_queries),
            blockify(chain_keys),
            blockify(chain_values),
            blockify(shrinkage_exponent),
        ),
    )
    local_out = local_out.reshape(row_count, linear_head_list, GLA_DV)
    carried_query = carried_query.reshape(row_count, linear_head_list, RECURRENT_DIM)
    own_decay = jnp.exp(log_total)
    carried_in = prefix(
        (own_decay, own_state),
        "sp",
        combine_chain,
        (jnp.ones_like(own_decay), jnp.zeros_like(own_state)),
    )[1]
    chain_full = local_out + jnp.einsum(
        "thd,hde->the", carried_query, carried_in, precision=HIGHEST
    )
    chain_out = (
        (rms_scale(chain_full, linear_norm_gain) * gated)
        .reshape(row_count, linear_head_list * GLA_DV)
        .astype(jnp.bfloat16)
    )
    return lax.psum_scatter(
        (
            jnp.dot(attn_out, differential_output_rows, preferred_element_type=jnp.float32)
            + jnp.dot(chain_out, linear_output_rows, preferred_element_type=jnp.float32)
        ).astype(jnp.bfloat16),
        "tp",
        scatter_dimension=0,
        tiled=True,
    )


def solution(mesh):
    placed = (
        P(("sp", "tp"), None),
        P(),
        P(None, "tp"),
        P(None, "tp"),
        P(None, "tp"),
        P(),
        P(),
        P("tp"),
        P(),
        P(None, "tp"),
        P(None, "tp"),
        P(None, "tp"),
        P(None, "tp"),
        P(),
        P(None, "tp"),
        P("tp"),
        P("sp", "tp"),
        P(),
        P("tp", None),
        P("tp", None),
    )
    return jax.shard_map(
        per_device, mesh=mesh, in_specs=placed, out_specs=P(("sp", "tp"), None), check_vma=False
    )
```

profile of v0, /device:TPU:0, one launch (start us, length us, event | category | flops | bytes accessed | tf_op | source)
XLA Modules:
  0.0 273.5 jit_solution(2683229393621899004)
XLA Ops:
  6.6 3.3 %constant_dynamic-update-slice_fusion.7 = bf16[2048,3104]{1,0:T(8,128)(2,1)} fusion(bf16[2048,512]{1,0:T(8,128)(2,1)} %param.30), kind=kLoop, calls=%fused_computation.130 | loop fusion | bytes 4194304
  10.5 2.4 all_gather.21
  13.0 3.2 %constant_dynamic-update-slice_fusion.6 = bf16[2048,3104]{1,0:T(8,128)(2,1)} fusion(bf16[2048,3104]{1,0:T(8,128)(2,1)} %constant_dynamic-update-slice_fusion.7, bf16[2048,512]{1,0:T(8,128)(2,1)} %param.31), kind=kLoop, calls=%fused_computation.129 | loop fusion | bytes 4194304
  23.9 8.3 %convolution_convert_fusion = bf16[128,3104]{0,1:T(8,128)(2,1)S(1)} fusion(bf16[128,2048]{1,0:T(8,128)(2,1)S(1)} %all_gather.21, bf16[2048,3104]{1,0:T(8,128)(2,1)} %constant_dynamic-update-slice_fusion), kind=kOutput, calls=%fused_computation.68 | convolution fusion | flops 1627787264 | bytes 14032896 | tf_op jit(solution)/shard_map/dot_general | solution.py:131
  41.0 1.8 reshape.219
  43.7 10.5 %while.8 = (s32[]{:T(128)}, f32[4,64,128]{2,1,0:T(8,128)S(1)}, f32[4,64]{1,0:T(4,128)S(1)}, f32[2,64,4,128]{3,1,0,2:T(8,128)}, f32[2,64,4,64]{3,2,1,0:T(4,128)},...) while((s32[]{:T(128)}, f32[4,64,128]{2,1,0:T(8,128)S(1)}, ...), condition=%wide.region_17.18_spmd.clone, body=%wide.region_15.0_spmd.clone.sunk | while | flops 89412096 | bytes 2970753 | solution.py:256
  55.6 2.9 %collective-permute-start = (bf16[64,512]{1,0:T(8,128)(2,1)S(1)}, bf16[64,512]{1,0:T(8,128)(2,1)S(1)}, u32[]{:S(2)}, u32[]{:S(2)}) collective-permute-start(bf16[64,512]{1,0:T(8,128)(2,1)S(1)} %reshape.212), channel_id=1, source_target_pairs={{0,2},{2,0},{4,6},{6,4},{8,10},{10,8},{12,14},{14,12},{16,18},{18,... | collective-permute-start | bytes 196616 | tf_op jit(solution)/shard_map/ppermute | solution.py:26
  58.5 2.4 collective-permute-done
  60.9 1.9 collective-permute-start.1
  65.8 40.7 %all-gather.2 = f32[16,4,64]{2,1,0:T(4,128)S(1)} all-gather(f32[1,4,64]{2,1,0:T(4,128)S(1)} %exponential_bitcast_fusion), channel_id=2, replica_groups=mesh['sp'=16,'tp'=2] {'sp'}, dimensions={0}, use_global_device_ids=true | all-gather | bytes 17408 | tf_op jit(solution)/shard_map/all_gather | solution.py:31
  106.6 4.3 %collective-permute-done.2 = bf16[64,512]{1,0:T(8,128)(2,1)S(1)} collective-permute-done((bf16[64,512]{1,0:T(8,128)(2,1)S(1)}, bf16[64,512]{1,0:T(8,128)(2,1)S(1)}, u32[]{:S(2)}, u32[]{:S(2)}) %collective-permute-start.2) | collective-permute-done | bytes 65568 | tf_op jit(solution)/shard_map/ppermute | solution.py:26
  110.9 52.9 %all-gather.9.cloned.1.call-done = bf16[2048,512]{0,1:T(8,128)(2,1)} async-done(((bf16[128,512]{0,1:T(8,128)(2,1)}), bf16[2048,512]{0,1:T(8,128)(2,1)}) %all-gather.9.cloned.1.call-update) | async-done | bytes 2097168 | tf_op jit(solution)/shard_map/all_gather | solution.py:171
  163.8 5.5 %conditional.3 = (f32[8,64]{1,0:T(8,128)S(1)}, f32[8,64,128]{2,1,0:T(8,128)S(1)}) conditional(s32[]{:T(128)} %convert_element_type.81, (f32[8,64]{1,0:T(8,128)S(1)}, f32[8,64,128]{2,1,0:T(8,128)S(1)}) %tuple.49, (s32[2048]{0:T(1024)S(1)}, s32[64]{0:T(128)S(1)}, bf16[64,512]{1,0:T(8,128)(2,1)S(1)}, bf16[2048,8,64]{0,2,1:T(8,128)(2,1)}, ...), branch_computations={%region_10.0_spmd, %region_11.0_spmd} | conditional | flops 412353536 | bytes 26839340 | solution.py:187
  164.3 2.6 fusion.9
  169.4 5.3 %conditional.2 = ((f32[8,64]{1,0:T(8,128)S(1)}, f32[8,64,128]{2,1,0:T(8,128)S(1)})) conditional(s32[]{:T(128)} %convert_element_type.71, (f32[8,64]{1,0:T(8,128)S(1)}, f32[8,64,128]{2,1,0:T(8,128)S(1)}) %tuple.49, (s32[2048]{0:T(1024)S(1)}, s32[64]{0:T(128)S(1)}, bf16[128,8,64]{2,0,1:T(8,128)(2,1)S(1)}, bf16[2048,8,64]{0,2,1:T(8,128)(2,1)}, ...), branch_computations={%region_4.5_spmd, %region_5.8_spmd} | conditional | flops 412353536 | bytes 26773812 | solution.py:187
  169.6 2.6 fusion.2
  177.4 47.9 %all-gather.11.cloned.1.call-done = f32[64,64,128]{2,1,0:T(8,128)} async-done(((f32[4,64,128]{2,1,0:T(8,128)}), f32[64,64,128]{2,1,0:T(8,128)}) %all-gather.11.cloned.1.call-update) | async-done | bytes 2097168 | tf_op jit(solution)/shard_map/all_gather | solution.py:31
  225.4 17.2 %while.9 = (s32[]{:T(128)}, f32[4,64,128]{2,1,0:T(8,128)S(1)}, s32[]{:T(128)}, f32[16,4,64]{2,1,0:T(4,128)S(1)}, f32[16,4,64,128]{3,2,1,0:T(8,128)}, /*index=5*/s32[]{:T(128)}, s32[]{:T(128)}) while((s32[]{:T(128)}, f32[4,64,128]{2,1,0:T(8,128)S(1)}, s32[]{:T(128)}, f32[16,4,64]{2,1,0:T(4,128)S(1)}, ...), condition=%wide.region_19.20_spmd.clone, body=%wide.region_18.19_spmd.clone.sunk | while | flops 131076 | bytes 396393 | solution.py:43
  242.7 1.7 multiply_reduce_fusion
  245.9 2.8 %collective-permute-done.5 = bf16[64,512]{1,0:T(8,128)(2,1)S(1)} collective-permute-done((bf16[64,512]{1,0:T(8,128)(2,1)S(1)}, bf16[64,512]{1,0:T(8,128)(2,1)S(1)}, u32[]{:S(2)}, u32[]{:S(2)}) %collective-permute-start.5) | collective-permute-done | bytes 65568 | tf_op jit(solution)/shard_map/ppermute | solution.py:26
  250.3 2.7 collective-permute-done.6
  253.0 1.8 collective-permute-start.7
  255.3 2.9 %collective-permute-done.7 = bf16[64,512]{1,0:T(8,128)(2,1)S(1)} collective-permute-done((bf16[64,512]{1,0:T(8,128)(2,1)S(1)}, bf16[64,512]{1,0:T(8,128)(2,1)S(1)}, u32[]{:S(2)}, u32[]{:S(2)}) %collective-permute-start.7) | collective-permute-done | bytes 65568 | tf_op jit(solution)/shard_map/ppermute | solution.py:26
  259.4 7.6 %reduce-scatter.2.cloned.1.call-done = bf16[64,2048]{1,0:T(8,128)(2,1)} async-done(((bf16[128,2048]{1,0:T(8,128)(2,1)}), bf16[64,2048]{1,0:T(8,128)(2,1)}) %reduce-scatter.2.cloned.1.call-update) | async-done | bytes 262160 | tf_op jit(solution)/shard_map/reduce_scatter | solution.py:283
  (192 shorter events, 61.0 us)
Async XLA Ops:
  6.5 248.2 %copy-start = (bf16[512,2048]{1,0:T(8,128)(2,1)S(1)}, bf16[512,2048]{1,0:T(8,128)(2,1)}, u32[]{:S(2)}) copy-start(bf16[512,2048]{1,0:T(8,128)(2,1)} %param.47) | copy-start | bytes 6291460
  6.5 104.3 %all-gather.7.cloned.1.call-start = ((), (), s32[]{:S(2)}) async-start(), calls=%async_computation.1 | async-start | bytes 2228224 | tf_op jit(solution)/shard_map/all_gather | solution.py:170
  10.2 6.0 %copy-start.4 = (bf16[2048,512]{1,0:T(8,128)(2,1)S(1)}, bf16[2048,512]{1,0:T(8,128)(2,1)}, u32[]{:S(2)}) copy-start(bf16[2048,512]{1,0:T(8,128)(2,1)} %param.32) | copy-start | bytes 6291460
  23.9 8.4 %copy-start.16 = (f32[64]{0:T(128)S(1)}, f32[64]{0:T(128)}, u32[]{:S(2)}) copy-start(f32[64]{0:T(128)} %param.34) | copy-start | bytes 772
  23.9 13.8 %copy-start.20 = (bf16[32,256]{1,0:T(8,128)(2,1)S(1)}, bf16[32,256]{1,0:T(8,128)(2,1)}, u32[]{:S(2)}) copy-start(bf16[32,256]{1,0:T(8,128)(2,1)} %param.42) | copy-start | bytes 49156
  23.9 13.9 %copy-start.21 = (f32[256]{0:T(256)S(1)}, f32[256]{0:T(256)}, u32[]{:S(2)}) copy-start(f32[256]{0:T(256)} %param.43) | copy-start | bytes 3076
  32.2 7.6 %copy-start.14 = (f32[128,4]{0,1:T(4,128)S(1)}, f32[128,4]{0,1:T(4,128)}, u32[]{:S(2)}) copy-start(f32[128,4]{0,1:T(4,128)} %param.44) | copy-start | bytes 6148
  33.3 130.5 %all-gather.9.cloned.1.call-start = ((), (), s32[]{:S(2)}) async-start(), calls=%async_computation.2 | async-start | bytes 2228224 | tf_op jit(solution)/shard_map/all_gather | solution.py:171
  34.1 191.3 %all-gather.11.cloned.1.call-start = ((), (), s32[]{:S(2)}) async-start(), calls=%async_computation.4 | async-start | bytes 2228224 | tf_op jit(solution)/shard_map/all_gather | solution.py:31
  43.7 11.4 %copy-start.17 = (f32[64]{0:T(128)S(1)}, f32[64]{0:T(128)}, u32[]{:S(2)}) copy-start(f32[64]{0:T(128)} %param.33) | copy-start | bytes 772
  54.9 212.2 %reduce-scatter.2.cloned.1.call-start = ((), (), s32[]{:S(2)}) async-start(), calls=%async_computation.3 | async-start | bytes 786432 | tf_op jit(solution)/shard_map/reduce_scatter | solution.py:283
  55.6 5.3 %collective-permute-start = (bf16[64,512]{1,0:T(8,128)(2,1)S(1)}, bf16[64,512]{1,0:T(8,128)(2,1)S(1)}, u32[]{:S(2)}, u32[]{:S(2)}) collective-permute-start(bf16[64,512]{1,0:T(8,128)(2,1)S(1)} %reshape.212), channel_id=1, source_target_pairs={{0,2},{2,0},{4,6},{6,4},{8,10},{10,8},{12,14},{14,12},{16,18},{18,... | collective-permute-start | bytes 196616 | tf_op jit(solution)/shard_map/ppermute | solution.py:26
  60.9 45.7 %collective-permute-start.1 = (bf16[64,512]{1,0:T(8,128)(2,1)S(1)}, bf16[64,512]{1,0:T(8,128)(2,1)S(1)}, u32[]{:S(2)}, u32[]{:S(2)}) collective-permute-start(bf16[64,512]{1,0:T(8,128)(2,1)S(1)} %collective-permute-done), channel_id=1, source_target_pairs={{0,4},{4,0},{2,6},{6,2},{8,12},{12,8},{10,14},{14,10},{16,20},{20,... | collective-permute-start | bytes 196616 | tf_op jit(solution)/shard_map/ppermute | solution.py:26
  106.6 4.3 %collective-permute-start.2 = (bf16[64,512]{1,0:T(8,128)(2,1)S(1)}, bf16[64,512]{1,0:T(8,128)(2,1)S(1)}, u32[]{:S(2)}, u32[]{:S(2)}) collective-permute-start(bf16[64,512]{1,0:T(8,128)(2,1)S(1)} %collective-permute-done.1), channel_id=1, source_target_pairs={{0,8},{8,0},{2,10},{10,2},{4,12},{12,4},{6,14},{14,6},{16,24},{24,... | collective-permute-start | bytes 196616 | tf_op jit(solution)/shard_map/ppermute | solution.py:26
  110.9 53.0 %collective-permute-start.3 = (bf16[64,512]{1,0:T(8,128)(2,1)S(1)}, bf16[64,512]{1,0:T(8,128)(2,1)S(1)}, u32[]{:S(2)}, u32[]{:S(2)}) collective-permute-start(bf16[64,512]{1,0:T(8,128)(2,1)S(1)} %collective-permute-done.2), channel_id=1, source_target_pairs={{0,16},{16,0},{2,18},{18,2},{4,20},{20,4},{6,22},{22,6},{8,24},{24... | collective-permute-start | bytes 196616 | tf_op jit(solution)/shard_map/ppermute | solution.py:26
  169.4 5.7 %copy-start.15 = (f32[4]{0:T(128)S(1)}, f32[4]{0:T(128)}, u32[]{:S(2)}) copy-start(f32[4]{0:T(128)} %param.35) | copy-start | bytes 52
  169.4 6.2 %copy-start.18 = (f32[128]{0:T(128)S(1)}, f32[128]{0:T(128)}, u32[]{:S(2)}) copy-start(f32[128]{0:T(128)} %param.36) | copy-start | bytes 1540
  174.7 75.5 %copy-start.11 = (f32[128,512]{0,1:T(8,128)S(1)}, f32[128,512]{0,1:T(8,128)}, u32[]{:S(2)}) copy-start(f32[128,512]{0,1:T(8,128)} %get-tuple-element.532) | copy-start | bytes 786436
  174.7 75.5 %copy-start.19 = (f32[128]{0:T(128)S(1)}, f32[128]{0:T(128)}, u32[]{:S(2)}) copy-start(f32[128]{0:T(128)} %param.45) | copy-start | bytes 1540
  176.0 68.4 %collective-permute-start.4 = (bf16[64,512]{1,0:T(8,128)(2,1)S(1)}, bf16[64,512]{1,0:T(8,128)(2,1)S(1)}, u32[]{:S(2)}, u32[]{:S(2)}) collective-permute-start(bf16[64,512]{1,0:T(8,128)(2,1)S(1)} %bitcast.194), channel_id=1, source_target_pairs={{0,2},{2,0},{4,6},{6,4},{8,10},{10,8},{12,14},{14,12},{16,18},{18,... | collective-permute-start | bytes 196616 | tf_op jit(solution)/shard_map/ppermute | solution.py:26
  242.6 15.5 %copy-start.7 = (bf16[512,2048]{1,0:T(8,128)(2,1)S(1)}, bf16[512,2048]{1,0:T(8,128)(2,1)}, u32[]{:S(2)}) copy-start(bf16[512,2048]{1,0:T(8,128)(2,1)} %param.46) | copy-start | bytes 6291460
  244.4 4.3 %collective-permute-start.5 = (bf16[64,512]{1,0:T(8,128)(2,1)S(1)}, bf16[64,512]{1,0:T(8,128)(2,1)S(1)}, u32[]{:S(2)}, u32[]{:S(2)}) collective-permute-start(bf16[64,512]{1,0:T(8,128)(2,1)S(1)} %collective-permute-done.4), channel_id=1, source_target_pairs={{0,4},{4,0},{2,6},{6,2},{8,12},{12,8},{10,14},{14,10},{16,20},{20,... | collective-permute-start | bytes 196616 | tf_op jit(solution)/shard_map/ppermute | solution.py:26
  248.7 4.3 %collective-permute-start.6 = (bf16[64,512]{1,0:T(8,128)(2,1)S(1)}, bf16[64,512]{1,0:T(8,128)(2,1)S(1)}, u32[]{:S(2)}, u32[]{:S(2)}) collective-permute-start(bf16[64,512]{1,0:T(8,128)(2,1)S(1)} %collective-permute-done.5), channel_id=1, source_target_pairs={{0,8},{8,0},{2,10},{10,2},{4,12},{12,4},{6,14},{14,6},{16,24},{24,... | collective-permute-start | bytes 196616 | tf_op jit(solution)/shard_map/ppermute | solution.py:26
  253.0 5.2 %collective-permute-start.7 = (bf16[64,512]{1,0:T(8,128)(2,1)S(1)}, bf16[64,512]{1,0:T(8,128)(2,1)S(1)}, u32[]{:S(2)}, u32[]{:S(2)}) collective-permute-start(bf16[64,512]{1,0:T(8,128)(2,1)S(1)} %collective-permute-done.6), channel_id=1, source_target_pairs={{0,16},{16,0},{2,18},{18,2},{4,20},{20,4},{6,22},{22,6},{8,24},{24... | collective-permute-start | bytes 196616 | tf_op jit(solution)/shard_map/ppermute | solution.py:26
  (10 other events, 29.7 us)
Sparse Core Ops, SparseCore 0:
  33.4 65.8 all-gather.6
  102.0 61.7 all-gather.8
  166.6 58.7 all-gather.10
  259.6 7.4 reduce-scatter.1
where the time goes:
time: 274 us
  waiting for transfers between devices  124 us (45%)
  blocking collectives  43.2 us (16%)
  other arithmetic  29.7 us (11%)
  local copies, waits for them, and re-layouts  27 us (10%)
  matrix products  23 us (8%)
  between operations  14.8 us (5%)
  starting transfers between devices  11.2 us (4%)
    all_gather x1, waiting for transfers between devices, per_device(): value_rows = lax.all_gather(value_flat, 'sp', axis=0, tiled=True)  52.9 us
    all_gather x1, waiting for transfers between devices, prefix(): everything = jax.tree.map(lambda part: lax.all_gather(part, axis), shard)  47.9 us
    all_gather x1, blocking collectives, prefix(): everything = jax.tree.map(lambda part: lax.all_gather(part, axis), shard)  40.7 us
    select_n x16, other arithmetic, turn(): return jax.tree.map(lambda a, b: jnp.where(reached, a, b), new, before)  16.6 us
    unnamed x52, local copies, waits for them, and re-layouts  15.6 us
    ppermute x8, waiting for transfers between devices, partner(): return lax.ppermute(block, axis, route)  15 us
    ppermute x8, starting transfers between devices, partner(): return lax.ppermute(block, axis, route)  11.1 us
    dot_general x1, matrix products, per_device(): jnp.dot(lax.all_gather(normed, 'tp', axis=0, tiled=True), packed, preferr...  8.26 us
  transfers between devices with their start and end apart: 12, of which 8 were waited for; matrix products, arithmetic and copies ran while one was open for 19% of the time, Pallas kernels for 0%

commit v1 on v0

--- a/solution.py
+++ b/solution.py
@@ -14,6 +14,21 @@
 OUT_SCALE = 0.8
 NEG_LARGE = -1e30
 HIGHEST = lax.Precision.HIGHEST
+
+
+def perform_cycles(t0, d0):
+    mesh_ax = "sp"
+    n_all = lax.axis_size(mesh_ax)
+    parts_out = sorted(((tick, (tick + 1) % n_all) for tick in range(n_all)))
+    r1 = t0
+    gallery = [r1]
+    q = 1
+    while q < n_all:
+        r1 = lax.ppermute(r1, axis_name=mesh_ax, perm=parts_out)
+        gallery.insert(0, r1)
+        q = q + 1
+    row_out = jnp.concatenate(gallery, d0)
+    return jnp.roll(row_out, (lax.axis_index(mesh_ax) + 1) * t0.shape[d0], d0)
 
 
 def partner(block, axis, apart):
@@ -168,7 +183,7 @@
         )
     )
     key_rows = lax.all_gather(key_flat, "sp", axis=0, tiled=True)
-    value_rows = lax.all_gather(value_flat, "sp", axis=0, tiled=True)
+    value_rows = perform_cycles(value_flat, 0)
     piece_rows = key_rows.shape[0]
     span_rows = block_length(piece_rows, row_count)
 

time: 274 us -> 316 us (1.15)
  local copies, waits for them, and re-layouts: 27 us -> 52 us
  waiting for transfers between devices: 124 us -> 148 us
  starting transfers between devices: 11.2 us -> 3.91 us
    ppermute x0 -> x15, waiting for transfers between devices: none -> 121 us  [perform_cycles(): r1 = lax.ppermute(r1, axis_name=mesh_ax, perm=parts_out)]
    all_gather x1 -> x0, waiting for transfers between devices: 52.9 us -> none  [per_device(): value_rows = lax.all_gather(value_flat, 'sp', axis=0, tiled=True)]
    all_gather x1, waiting for transfers between devices: 47.9 us -> 0.02 us  [prefix(): everything = jax.tree.map(lambda part: lax.all_gather(part, axis), shard)]
    unnamed x52 -> x131, local copies, waits for them, and re-layouts: 15.6 us -> 37.9 us
    ppermute x8, starting transfers between devices: 11.1 us -> 0.85 us  [partner(): return lax.ppermute(block, axis, route)]
    ppermute x8, waiting for transfers between devices: 15 us -> 21 us  [partner(): return lax.ppermute(block, axis, route)]
  transfers between devices with their start and end apart: 12 -> 26, of which waited for: 8 -> 22; matrix products, arithmetic and copies ran while one was open for 19% -> 23% of each run, Pallas kernels for 0% -> 0%
where the time goes in v1:
time: 316 us; the launch traced here: 315 us
  waiting for transfers between devices  148 us (47%)
  local copies, waits for them, and re-layouts  52 us (16%)
  blocking collectives  41 us (13%)
  other arithmetic  31.3 us (10%)
  matrix products  22.1 us (7%)
  between operations  15.4 us (5%)
  starting transfers between devices  3.91 us (1%)
    ppermute x15, waiting for transfers between devices, perform_cycles(): r1 = lax.ppermute(r1, axis_name=mesh_ax, perm=parts_out)  121 us
    all_gather x1, blocking collectives, prefix(): everything = jax.tree.map(lambda part: lax.all_gather(part, axis), shard)  38.6 us
    unnamed x131, local copies, waits for them, and re-layouts  37.9 us
    ppermute x8, waiting for transfers between devices, partner(): return lax.ppermute(block, axis, route)  21 us
    select_n x16, other arithmetic, turn(): return jax.tree.map(lambda a, b: jnp.where(reached, a, b), new, before)  16.6 us
    dot_general x1, matrix products, per_device(): jnp.dot(lax.all_gather(normed, 'tp', axis=0, tiled=True), packed, preferr...  8.26 us
    reduce_scatter x1, waiting for transfers between devices, per_device(): lax.psum_scatter((jnp.dot(attn_out, differential_output_rows, preferred_e...  6.71 us
  transfers between devices with their start and end apart: 26, of which 22 were waited for; matrix products, arithmetic and copies ran while one was open for 23% of the time, Pallas kernels for 0%

profile of v1, /device:TPU:0, one launch (start us, length us, event | category | flops | bytes accessed | tf_op | source)
XLA Modules:
  0.0 314.9 jit_solution(1062680917573021336)
XLA Ops:
  24.0 8.3 %convolution_convert_fusion = bf16[128,3104]{0,1:T(8,128)(2,1)S(1)} fusion(bf16[128,2048]{1,0:T(8,128)(2,1)S(1)} %all_gather.18, bf16[2048,3104]{1,0:T(8,128)(2,1)} %constant_dynamic-update-slice_fusion), kind=kOutput, calls=%fused_computation.68 | convolution fusion | flops 1627787264 | bytes 14032896 | tf_op jit(solution)/shard_map/dot_general | solution.py:146
  35.1 7.8 %collective-permute-done = bf16[128,512]{0,1:T(8,128)(2,1)S(1)} collective-permute-done((bf16[128,512]{0,1:T(8,128)(2,1)S(1)}, bf16[128,512]{0,1:T(8,128)(2,1)S(1)}, u32[]{:S(2)}, u32[]{:S(2)}) %collective-permute-start) | collective-permute-done | bytes 131104 | tf_op jit(solution)/shard_map/ppermute | solution.py:27
  43.6 8.6 %collective-permute-done.1 = bf16[128,512]{0,1:T(8,128)(2,1)S(1)} collective-permute-done((bf16[128,512]{0,1:T(8,128)(2,1)S(1)}, bf16[128,512]{0,1:T(8,128)(2,1)S(1)}, u32[]{:S(2)}, u32[]{:S(2)}) %collective-permute-start.1) | collective-permute-done | bytes 131104 | tf_op jit(solution)/shard_map/ppermute | solution.py:27
  52.8 8.6 %collective-permute-done.2 = bf16[128,512]{0,1:T(8,128)(2,1)S(1)} collective-permute-done((bf16[128,512]{0,1:T(8,128)(2,1)S(1)}, bf16[128,512]{0,1:T(8,128)(2,1)S(1)}, u32[]{:S(2)}, u32[]{:S(2)}) %collective-permute-start.2) | collective-permute-done | bytes 131104 | tf_op jit(solution)/shard_map/ppermute | solution.py:27
  62.0 8.6 %collective-permute-done.3 = bf16[128,512]{0,1:T(8,128)(2,1)S(1)} collective-permute-done((bf16[128,512]{0,1:T(8,128)(2,1)S(1)}, bf16[128,512]{0,1:T(8,128)(2,1)S(1)}, u32[]{:S(2)}, u32[]{:S(2)}) %collective-permute-start.3) | collective-permute-done | bytes 131104 | tf_op jit(solution)/shard_map/ppermute | solution.py:27
  71.2 8.6 %collective-permute-done.4 = bf16[128,512]{0,1:T(8,128)(2,1)S(1)} collective-permute-done((bf16[128,512]{0,1:T(8,128)(2,1)S(1)}, bf16[128,512]{0,1:T(8,128)(2,1)S(1)}, u32[]{:S(2)}, u32[]{:S(2)}) %collective-permute-start.4) | collective-permute-done | bytes 131104 | tf_op jit(solution)/shard_map/ppermute | solution.py:27
  80.5 8.6 %collective-permute-done.5 = bf16[128,512]{0,1:T(8,128)(2,1)S(1)} collective-permute-done((bf16[128,512]{0,1:T(8,128)(2,1)S(1)}, bf16[128,512]{0,1:T(8,128)(2,1)S(1)}, u32[]{:S(2)}, u32[]{:S(2)}) %collective-permute-start.5) | collective-permute-done | bytes 131104 | tf_op jit(solution)/shard_map/ppermute | solution.py:27
  89.7 9.1 %collective-permute-done.6 = bf16[128,512]{0,1:T(8,128)(2,1)S(1)} collective-permute-done((bf16[128,512]{0,1:T(8,128)(2,1)S(1)}, bf16[128,512]{0,1:T(8,128)(2,1)S(1)}, u32[]{:S(2)}, u32[]{:S(2)}) %collective-permute-start.6) | collective-permute-done | bytes 131104 | tf_op jit(solution)/shard_map/ppermute | solution.py:27
  99.4 9.7 %collective-permute-done.7 = bf16[128,512]{0,1:T(8,128)(2,1)S(1)} collective-permute-done((bf16[128,512]{0,1:T(8,128)(2,1)S(1)}, bf16[128,512]{0,1:T(8,128)(2,1)S(1)}, u32[]{:S(2)}, u32[]{:S(2)}) %collective-permute-start.7) | collective-permute-done | bytes 131104 | tf_op jit(solution)/shard_map/ppermute | solution.py:27
  109.8 8.6 %collective-permute-done.8 = bf16[128,512]{0,1:T(8,128)(2,1)S(1)} collective-permute-done((bf16[128,512]{0,1:T(8,128)(2,1)S(1)}, bf16[128,512]{0,1:T(8,128)(2,1)S(1)}, u32[]{:S(2)}, u32[]{:S(2)}) %collective-permute-start.8) | collective-permute-done | bytes 131104 | tf_op jit(solution)/shard_map/ppermute | solution.py:27
  118.5 8.4 %collective-permute-done.9 = bf16[128,512]{0,1:T(8,128)(2,1)S(1)} collective-permute-done((bf16[128,512]{0,1:T(8,128)(2,1)S(1)}, bf16[128,512]{0,1:T(8,128)(2,1)S(1)}, u32[]{:S(2)}, u32[]{:S(2)}) %collective-permute-start.9) | collective-permute-done | bytes 131104 | tf_op jit(solution)/shard_map/ppermute | solution.py:27
  128.0 7.5 %collective-permute-done.10 = bf16[128,512]{0,1:T(8,128)(2,1)S(1)} collective-permute-done((bf16[128,512]{0,1:T(8,128)(2,1)S(1)}, bf16[128,512]{0,1:T(8,128)(2,1)S(1)}, u32[]{:S(2)}, u32[]{:S(2)}) %collective-permute-start.10) | collective-permute-done | bytes 131104 | tf_op jit(solution)/shard_map/ppermute | solution.py:27
  138.9 5.4 %collective-permute-done.11 = bf16[128,512]{0,1:T(8,128)(2,1)} collective-permute-done((bf16[128,512]{0,1:T(8,128)(2,1)S(1)}, bf16[128,512]{0,1:T(8,128)(2,1)}, u32[]{:S(2)}, u32[]{:S(2)}) %collective-permute-start.11) | collective-permute-done | bytes 131104 | tf_op jit(solution)/shard_map/ppermute | solution.py:27
  146.0 7.1 %collective-permute-done.12 = bf16[128,512]{0,1:T(8,128)(2,1)} collective-permute-done((bf16[128,512]{0,1:T(8,128)(2,1)}, bf16[128,512]{0,1:T(8,128)(2,1)}, u32[]{:S(2)}, u32[]{:S(2)}) %collective-permute-start.12) | collective-permute-done | bytes 131104 | tf_op jit(solution)/shard_map/ppermute | solution.py:27
  155.7 7.2 %collective-permute-done.13 = bf16[128,512]{0,1:T(8,128)(2,1)} collective-permute-done((bf16[128,512]{0,1:T(8,128)(2,1)}, bf16[128,512]{0,1:T(8,128)(2,1)}, u32[]{:S(2)}, u32[]{:S(2)}) %collective-permute-start.13) | collective-permute-done | bytes 131104 | tf_op jit(solution)/shard_map/ppermute | solution.py:27
  164.7 7.0 %collective-permute-done.14 = bf16[128,512]{0,1:T(8,128)(2,1)S(1)} collective-permute-done((bf16[128,512]{0,1:T(8,128)(2,1)}, bf16[128,512]{0,1:T(8,128)(2,1)S(1)}, u32[]{:S(2)}, u32[]{:S(2)}) %collective-permute-start.14) | collective-permute-done | bytes 131104 | tf_op jit(solution)/shard_map/ppermute | solution.py:27
  191.0 10.5 %while.8 = (s32[]{:T(128)}, f32[4,64,128]{2,1,0:T(8,128)S(1)}, f32[4,64]{1,0:T(4,128)S(1)}, f32[2,64,4,128]{3,1,0,2:T(8,128)}, f32[2,64,4,64]{3,2,1,0:T(4,128)},...) while((s32[]{:T(128)}, f32[4,64,128]{2,1,0:T(8,128)S(1)}, ...), condition=%wide.region_17.18_spmd.clone, body=%wide.region_15.17_spmd.clone.sunk | while | flops 89412096 | bytes 2970753 | solution.py:271
  207.8 4.3 %collective-permute-done.16 = bf16[64,512]{1,0:T(8,128)(2,1)S(1)} collective-permute-done((bf16[64,512]{1,0:T(8,128)(2,1)S(1)}, bf16[64,512]{1,0:T(8,128)(2,1)S(1)}, u32[]{:S(2)}, u32[]{:S(2)}) %collective-permute-start.16) | collective-permute-done | bytes 65568 | tf_op jit(solution)/shard_map/ppermute | solution.py:41
  212.1 4.7 %collective-permute-done.17 = bf16[64,512]{1,0:T(8,128)(2,1)S(1)} collective-permute-done((bf16[64,512]{1,0:T(8,128)(2,1)S(1)}, bf16[64,512]{1,0:T(8,128)(2,1)S(1)}, u32[]{:S(2)}, u32[]{:S(2)}) %collective-permute-start.17) | collective-permute-done | bytes 65568 | tf_op jit(solution)/shard_map/ppermute | solution.py:41
  221.9 5.4 %conditional.3 = (f32[8,64]{1,0:T(8,128)S(1)}, f32[8,64,128]{2,1,0:T(8,128)S(1)}) conditional(s32[]{:T(128)} %convert_element_type.81, (f32[8,64]{1,0:T(8,128)S(1)}, f32[8,64,128]{2,1,0:T(8,128)S(1)}) %tuple.49, (s32[2048]{0:T(1024)S(1)}, s32[64]{0:T(128)S(1)}, bf16[64,512]{1,0:T(8,128)(2,1)S(1)}, bf16[2048,8,64]{0,2,1:T(8,128)(2,1)}, ...), branch_computations={%region_10.11_spmd, %region_11.14_spmd} | conditional | flops 412353536 | bytes 26839340 | solution.py:202
  227.4 5.3 %conditional.2 = ((f32[8,64]{1,0:T(8,128)S(1)}, f32[8,64,128]{2,1,0:T(8,128)S(1)})) conditional(s32[]{:T(128)} %convert_element_type.71, (f32[8,64]{1,0:T(8,128)S(1)}, f32[8,64,128]{2,1,0:T(8,128)S(1)}) %tuple.49, (s32[2048]{0:T(1024)S(1)}, s32[64]{0:T(128)S(1)}, bf16[128,8,64]{2,0,1:T(8,128)(2,1)S(1)}, bf16[2048,8,64]{0,2,1:T(8,128)(2,1)}, ...), branch_computations={%region_4.5_spmd, %region_5.0_spmd} | conditional | flops 412353536 | bytes 26773812 | solution.py:202
  242.8 38.6 %all-gather.2 = f32[16,4,64]{2,1,0:T(4,128)S(1)} all-gather(f32[1,4,64]{2,1,0:T(4,128)S(1)} %exponential_bitcast_fusion), channel_id=2, replica_groups=mesh['sp'=16,'tp'=2] {'sp'}, dimensions={0}, use_global_device_ids=true | all-gather | bytes 17408 | tf_op jit(solution)/shard_map/all_gather | solution.py:46
  281.5 17.3 %while.9 = (s32[]{:T(128)}, f32[4,64,128]{2,1,0:T(8,128)S(1)}, s32[]{:T(128)}, f32[16,4,64]{2,1,0:T(4,128)S(1)}, f32[16,4,64,128]{3,2,1,0:T(8,128)}, /*index=5*/s32[]{:T(128)}, s32[]{:T(128)}) while((s32[]{:T(128)}, f32[4,64,128]{2,1,0:T(8,128)S(1)}, s32[]{:T(128)}, f32[16,4,64]{2,1,0:T(4,128)S(1)}, ...), condition=%wide.region_19.20_spmd.clone, body=%wide.region_18.19_spmd.clone.sunk | while | flops 131076 | bytes 396393 | solution.py:58
  301.6 6.7 %reduce-scatter.2.cloned.1.call-done = bf16[64,2048]{1,0:T(8,128)(2,1)} async-done(((bf16[128,2048]{1,0:T(8,128)(2,1)}), bf16[64,2048]{1,0:T(8,128)(2,1)}) %reduce-scatter.2.cloned.1.call-update) | async-done | bytes 262160 | tf_op jit(solution)/shard_map/reduce_scatter | solution.py:298
  (300 shorter events, 115.6 us)
Async XLA Ops:
  6.5 213.4 %all-gather.6.cloned.1.call-start = ((), (), s32[]{:S(2)}) async-start(), calls=%async_computation.1 | async-start | bytes 2228224 | tf_op jit(solution)/shard_map/all_gather | solution.py:185
  32.2 10.7 %collective-permute-start = (bf16[128,512]{0,1:T(8,128)(2,1)S(1)}, bf16[128,512]{0,1:T(8,128)(2,1)S(1)}, u32[]{:S(2)}, u32[]{:S(2)}) collective-permute-start(bf16[128,512]{0,1:T(8,128)(2,1)S(1)} %slice.63), channel_id=1, source_target_pairs={{0,2},{2,4},{4,6},{6,8},{8,10},{10,12},{12,14},{14,16},{16,18},{18... | collective-permute-start | bytes 393224 | tf_op jit(solution)/shard_map/ppermute | solution.py:27
  43.6 8.6 %collective-permute-start.1 = (bf16[128,512]{0,1:T(8,128)(2,1)S(1)}, bf16[128,512]{0,1:T(8,128)(2,1)S(1)}, u32[]{:S(2)}, u32[]{:S(2)}) collective-permute-start(bf16[128,512]{0,1:T(8,128)(2,1)S(1)} %collective-permute-done), channel_id=1, source_target_pairs={{0,2},{2,4},{4,6},{6,8},{8,10},{10,12},{12,14},{14,16},{16,18},{18... | collective-permute-start | bytes 393224 | tf_op jit(solution)/shard_map/ppermute | solution.py:27
  52.8 8.6 %collective-permute-start.2 = (bf16[128,512]{0,1:T(8,128)(2,1)S(1)}, bf16[128,512]{0,1:T(8,128)(2,1)S(1)}, u32[]{:S(2)}, u32[]{:S(2)}) collective-permute-start(bf16[128,512]{0,1:T(8,128)(2,1)S(1)} %collective-permute-done.1), channel_id=1, source_target_pairs={{0,2},{2,4},{4,6},{6,8},{8,10},{10,12},{12,14},{14,16},{16,18},{18... | collective-permute-start | bytes 393224 | tf_op jit(solution)/shard_map/ppermute | solution.py:27
  62.0 8.6 %collective-permute-start.3 = (bf16[128,512]{0,1:T(8,128)(2,1)S(1)}, bf16[128,512]{0,1:T(8,128)(2,1)S(1)}, u32[]{:S(2)}, u32[]{:S(2)}) collective-permute-start(bf16[128,512]{0,1:T(8,128)(2,1)S(1)} %collective-permute-done.2), channel_id=1, source_target_pairs={{0,2},{2,4},{4,6},{6,8},{8,10},{10,12},{12,14},{14,16},{16,18},{18... | collective-permute-start | bytes 393224 | tf_op jit(solution)/shard_map/ppermute | solution.py:27
  71.2 8.6 %collective-permute-start.4 = (bf16[128,512]{0,1:T(8,128)(2,1)S(1)}, bf16[128,512]{0,1:T(8,128)(2,1)S(1)}, u32[]{:S(2)}, u32[]{:S(2)}) collective-permute-start(bf16[128,512]{0,1:T(8,128)(2,1)S(1)} %collective-permute-done.3), channel_id=1, source_target_pairs={{0,2},{2,4},{4,6},{6,8},{8,10},{10,12},{12,14},{14,16},{16,18},{18... | collective-permute-start | bytes 393224 | tf_op jit(solution)/shard_map/ppermute | solution.py:27
  80.5 8.6 %collective-permute-start.5 = (bf16[128,512]{0,1:T(8,128)(2,1)S(1)}, bf16[128,512]{0,1:T(8,128)(2,1)S(1)}, u32[]{:S(2)}, u32[]{:S(2)}) collective-permute-start(bf16[128,512]{0,1:T(8,128)(2,1)S(1)} %collective-permute-done.4), channel_id=1, source_target_pairs={{0,2},{2,4},{4,6},{6,8},{8,10},{10,12},{12,14},{14,16},{16,18},{18... | collective-permute-start | bytes 393224 | tf_op jit(solution)/shard_map/ppermute | solution.py:27
  89.7 9.1 %collective-permute-start.6 = (bf16[128,512]{0,1:T(8,128)(2,1)S(1)}, bf16[128,512]{0,1:T(8,128)(2,1)S(1)}, u32[]{:S(2)}, u32[]{:S(2)}) collective-permute-start(bf16[128,512]{0,1:T(8,128)(2,1)S(1)} %collective-permute-done.5), channel_id=1, source_target_pairs={{0,2},{2,4},{4,6},{6,8},{8,10},{10,12},{12,14},{14,16},{16,18},{18... | collective-permute-start | bytes 393224 | tf_op jit(solution)/shard_map/ppermute | solution.py:27
  99.4 9.7 %collective-permute-start.7 = (bf16[128,512]{0,1:T(8,128)(2,1)S(1)}, bf16[128,512]{0,1:T(8,128)(2,1)S(1)}, u32[]{:S(2)}, u32[]{:S(2)}) collective-permute-start(bf16[128,512]{0,1:T(8,128)(2,1)S(1)} %collective-permute-done.6), channel_id=1, source_target_pairs={{0,2},{2,4},{4,6},{6,8},{8,10},{10,12},{12,14},{14,16},{16,18},{18... | collective-permute-start | bytes 393224 | tf_op jit(solution)/shard_map/ppermute | solution.py:27
  109.8 8.6 %collective-permute-start.8 = (bf16[128,512]{0,1:T(8,128)(2,1)S(1)}, bf16[128,512]{0,1:T(8,128)(2,1)S(1)}, u32[]{:S(2)}, u32[]{:S(2)}) collective-permute-start(bf16[128,512]{0,1:T(8,128)(2,1)S(1)} %collective-permute-done.7), channel_id=1, source_target_pairs={{0,2},{2,4},{4,6},{6,8},{8,10},{10,12},{12,14},{14,16},{16,18},{18... | collective-permute-start | bytes 393224 | tf_op jit(solution)/shard_map/ppermute | solution.py:27
  118.4 8.6 %collective-permute-start.9 = (bf16[128,512]{0,1:T(8,128)(2,1)S(1)}, bf16[128,512]{0,1:T(8,128)(2,1)S(1)}, u32[]{:S(2)}, u32[]{:S(2)}) collective-permute-start(bf16[128,512]{0,1:T(8,128)(2,1)S(1)} %collective-permute-done.8), channel_id=1, source_target_pairs={{0,2},{2,4},{4,6},{6,8},{8,10},{10,12},{12,14},{14,16},{16,18},{18... | collective-permute-start | bytes 393224 | tf_op jit(solution)/shard_map/ppermute | solution.py:27
  126.9 8.6 %collective-permute-start.10 = (bf16[128,512]{0,1:T(8,128)(2,1)S(1)}, bf16[128,512]{0,1:T(8,128)(2,1)S(1)}, u32[]{:S(2)}, u32[]{:S(2)}) collective-permute-start(bf16[128,512]{0,1:T(8,128)(2,1)S(1)} %collective-permute-done.9), channel_id=1, source_target_pairs={{0,2},{2,4},{4,6},{6,8},{8,10},{10,12},{12,14},{14,16},{16,18},{18... | collective-permute-start | bytes 393224 | tf_op jit(solution)/shard_map/ppermute | solution.py:27
  127.9 153.6 %all-gather.8.cloned.1.call-start = ((), (), s32[]{:S(2)}) async-start(), calls=%async_computation.3 | async-start | bytes 2228224 | tf_op jit(solution)/shard_map/all_gather | solution.py:46
  135.5 8.8 %collective-permute-start.11 = (bf16[128,512]{0,1:T(8,128)(2,1)S(1)}, bf16[128,512]{0,1:T(8,128)(2,1)}, u32[]{:S(2)}, u32[]{:S(2)}) collective-permute-start(bf16[128,512]{0,1:T(8,128)(2,1)S(1)} %collective-permute-done.10), channel_id=1, source_target_pairs={{0,2},{2,4},{4,6},{6,8},{8,10},{10,12},{12,14},{14,16},{16,18},{18... | collective-permute-start | bytes 393224 | tf_op jit(solution)/shard_map/ppermute | solution.py:27
  144.3 8.9 %collective-permute-start.12 = (bf16[128,512]{0,1:T(8,128)(2,1)}, bf16[128,512]{0,1:T(8,128)(2,1)}, u32[]{:S(2)}, u32[]{:S(2)}) collective-permute-start(bf16[128,512]{0,1:T(8,128)(2,1)} %collective-permute-done.11), channel_id=1, source_target_pairs={{0,2},{2,4},{4,6},{6,8},{8,10},{10,12},{12,14},{14,16},{16,18},{18... | collective-permute-start | bytes 393224 | tf_op jit(solution)/shard_map/ppermute | solution.py:27
  153.1 9.8 %collective-permute-start.13 = (bf16[128,512]{0,1:T(8,128)(2,1)}, bf16[128,512]{0,1:T(8,128)(2,1)}, u32[]{:S(2)}, u32[]{:S(2)}) collective-permute-start(bf16[128,512]{0,1:T(8,128)(2,1)} %collective-permute-done.12), channel_id=1, source_target_pairs={{0,2},{2,4},{4,6},{6,8},{8,10},{10,12},{12,14},{14,16},{16,18},{18... | collective-permute-start | bytes 393224 | tf_op jit(solution)/shard_map/ppermute | solution.py:27
  162.9 8.8 %collective-permute-start.14 = (bf16[128,512]{0,1:T(8,128)(2,1)}, bf16[128,512]{0,1:T(8,128)(2,1)S(1)}, u32[]{:S(2)}, u32[]{:S(2)}) collective-permute-start(bf16[128,512]{0,1:T(8,128)(2,1)} %collective-permute-done.13), channel_id=1, source_target_pairs={{0,2},{2,4},{4,6},{6,8},{8,10},{10,12},{12,14},{14,16},{16,18},{18... | collective-permute-start | bytes 393224 | tf_op jit(solution)/shard_map/ppermute | solution.py:27
  202.1 106.2 %reduce-scatter.2.cloned.1.call-start = ((), (), s32[]{:S(2)}) async-start(), calls=%async_computation.2 | async-start | bytes 786432 | tf_op jit(solution)/shard_map/reduce_scatter | solution.py:298
  203.5 4.3 %collective-permute-start.15 = (bf16[64,512]{1,0:T(8,128)(2,1)S(1)}, bf16[64,512]{1,0:T(8,128)(2,1)S(1)}, u32[]{:S(2)}, u32[]{:S(2)}) collective-permute-start(bf16[64,512]{1,0:T(8,128)(2,1)S(1)} %reshape.212), channel_id=1, source_target_pairs={{0,2},{2,0},{4,6},{6,4},{8,10},{10,8},{12,14},{14,12},{16,18},{18,... | collective-permute-start | bytes 196616 | tf_op jit(solution)/shard_map/ppermute | solution.py:41
  212.1 4.7 %collective-permute-start.17 = (bf16[64,512]{1,0:T(8,128)(2,1)S(1)}, bf16[64,512]{1,0:T(8,128)(2,1)S(1)}, u32[]{:S(2)}, u32[]{:S(2)}) collective-permute-start(bf16[64,512]{1,0:T(8,128)(2,1)S(1)} %collective-permute-done.16), channel_id=1, source_target_pairs={{0,8},{8,0},{2,10},{10,2},{4,12},{12,4},{6,14},{14,6},{16,24},{24,... | collective-permute-start | bytes 196616 | tf_op jit(solution)/shard_map/ppermute | solution.py:41
  216.8 5.2 %collective-permute-start.18 = (bf16[64,512]{1,0:T(8,128)(2,1)S(1)}, bf16[64,512]{1,0:T(8,128)(2,1)S(1)}, u32[]{:S(2)}, u32[]{:S(2)}) collective-permute-start(bf16[64,512]{1,0:T(8,128)(2,1)S(1)} %collective-permute-done.17), channel_id=1, source_target_pairs={{0,16},{16,0},{2,18},{18,2},{4,20},{20,4},{6,22},{22,6},{8,24},{24... | collective-permute-start | bytes 196616 | tf_op jit(solution)/shard_map/ppermute | solution.py:41
  234.0 4.4 %collective-permute-start.19 = (bf16[64,512]{1,0:T(8,128)(2,1)S(1)}, bf16[64,512]{1,0:T(8,128)(2,1)S(1)}, u32[]{:S(2)}, u32[]{:S(2)}) collective-permute-start(bf16[64,512]{1,0:T(8,128)(2,1)S(1)} %bitcast.194), channel_id=1, source_target_pairs={{0,2},{2,0},{4,6},{6,4},{8,10},{10,8},{12,14},{14,12},{16,18},{18,... | collective-permute-start | bytes 196616 | tf_op jit(solution)/shard_map/ppermute | solution.py:41
  242.6 38.8 %collective-permute-start.21 = (bf16[64,512]{1,0:T(8,128)(2,1)S(1)}, bf16[64,512]{1,0:T(8,128)(2,1)}, u32[]{:S(2)}, u32[]{:S(2)}) collective-permute-start(bf16[64,512]{1,0:T(8,128)(2,1)S(1)} %collective-permute-done.20), channel_id=1, source_target_pairs={{0,8},{8,0},{2,10},{10,2},{4,12},{12,4},{6,14},{14,6},{16,24},{24,... | collective-permute-start | bytes 196616 | tf_op jit(solution)/shard_map/ppermute | solution.py:41
  281.4 18.7 %collective-permute-start.22 = (bf16[64,512]{1,0:T(8,128)(2,1)}, bf16[64,512]{1,0:T(8,128)(2,1)S(1)}, u32[]{:S(2)}, u32[]{:S(2)}) collective-permute-start(bf16[64,512]{1,0:T(8,128)(2,1)} %collective-permute-done.21), channel_id=1, source_target_pairs={{0,16},{16,0},{2,18},{18,2},{4,20},{20,4},{6,22},{22,6},{8,24},{24... | collective-permute-start | bytes 196616 | tf_op jit(solution)/shard_map/ppermute | solution.py:41
  (48 other events, 1283.1 us)
Sparse Core Ops, SparseCore 0:
  128.0 66.5 all-gather.5
  202.3 57.6 all-gather.7
  301.8 6.5 reduce-scatter.1
